TPU v7x, 128 devices: a whole 4x4x4 slice. The times are simulated.
128 devices in a mesh: rep: 2 (over z_hi), fs: 32 (over z_lo, y, x), tp: 2 (over core).
Axes of the slice: x: 4, y: 4, z: 4 (z_hi: 2, z_lo: 2; z = z_hi * 2 + z_lo), core: 2. Of those that a mesh axis runs over, the one named last changes fastest.
Arguments:
- tokens: bfloat16 [40960, 2048], P(('rep', 'fs'), 'tp'), may hold values from -6 to 6
- norm_first: float32 [2048], replicated, may hold values from 0.1 to 1.9
- norm_mix: float32 [2048], replicated, may hold values from 0.1 to 1.9
- norm_second: float32 [2048], replicated, may hold values from 0.1 to 1.9
- gate_weight: float32 [2048, 2816], P('fs', 'tp'), may hold values from -0.125 to 0.125
- up_weight: float32 [2048, 2816], P('fs', 'tp'), may hold values from -0.125 to 0.125
- down_weight: float32 [2816, 2048], P('tp', 'fs'), may hold values from -0.109375 to 0.109375
- gate_scale: float32 [2816], P('tp'), may hold values from 0.3 to 3
- up_scale: float32 [2816], P('tp'), may hold values from 0.3 to 3
- down_scale: float32 [2048], P('fs'), may hold values from 0.3 to 3
- u_weight: float32 [2048, 1024], P('fs', 'tp'), may hold values from -0.125 to 0.125
- v_weight: float32 [2048, 1024], P('fs', 'tp'), may hold values from -0.125 to 0.125
- u_scale: float32 [1024], P('tp'), may hold values from 0.3 to 3
- v_scale: float32 [1024], P('tp'), may hold values from 0.15 to 6
- ln_gain: float32 [1024], P('tp'), may hold values from 0.1 to 1.9
- ln_bias: float32 [1024], P('tp'), may hold values from -3 to 3
- spatial_weight: bfloat16 [8, 128, 128], P('tp'), may hold values from -0.25 to 0.25
- spatial_bias: float32 [8, 128], P('tp'), may hold values from 0.1 to 1.9
- out_weight: float32 [1024, 2048], P('tp', 'fs'), may hold values from -0.1875 to 0.1875
- out_scale: float32 [2048], P('fs'), may hold values from 0.3 to 3
Outputs:
- layer_out: bfloat16 [40960, 2048], P(('rep', 'fs'), 'tp')
All inputs are finite; a program needn't handle non-finite values.
Results may differ from a plain program's by a relative error of at most 0.019.
Values may be sent and summed in bfloat16 or wider, within the bound.
No kernel may reach another device: no remote copies, remote signals or barrier semaphores. Data moves between devices by JAX's collectives and lax.ppermute only.
A program may use at most 128 MiB of HBM per device.

v0:
```python
import jax
import jax.numpy as jnp
from jax import lax
from jax.sharding import Mesh
from jax.sharding import PartitionSpec as P

BW = 1024
SPAN = 128
FS = ("fs_0", "fs_1", "fs_2")
REP_FS = ("rep", "fs_0", "fs_1", "fs_2")


EPS = 1e-06


def rows_first(arrays, axis, dims):
    turned = [jnp.moveaxis(a, dim, 0) for a, dim in zip(arrays, dims)]
    both = jnp.concatenate([t.reshape(len(t), -1) for t in turned], axis=1)
    result, at, done = (lax.all_gather(both, axis, axis=0, tiled=True), 0, [])
    for t, dim in zip(turned, dims):
        slab = result[:, at : at + t[0].size].reshape(-1, *t.shape[1:])
        done.append(jnp.moveaxis(slab, 0, dim))
        at += t[0].size
    return tuple(done)


def sent_to_all(x, axis):
    size = lax.axis_size(axis)
    return lax.all_to_all(jnp.broadcast_to(x[None], (size, *x.shape)), axis, 0, 0, tiled=True)


def in_order(parts, dim):
    dims = list(parts.shape[1:])
    dims[dim] *= parts.shape[0]
    return jnp.moveaxis(parts, 0, dim).reshape(dims)


def gather_directly(x, axis, dim):
    parts = sent_to_all(x, axis)
    return in_order(parts, dim)


def cut_along(x, dim, size):
    dims = x.shape
    parts = x.reshape(*dims[:dim], size, dims[dim] // size, *dims[dim + 1 :])
    return jnp.moveaxis(parts, dim, 0)


def sum_at_owner(x, axis, dim):
    parts = cut_along(x, dim, lax.axis_size(axis))
    arrived = lax.all_to_all(parts, axis, split_axis=0, concat_axis=0, tiled=True)
    return arrived.astype(jnp.float32).sum(axis=0)


def sent_together(arrays, axis, dim, along):
    ends, at = ([], 0)
    for a in arrays[:-1]:
        at += a.shape[along]
        ends.append(at)
    both = jnp.concatenate(arrays, axis=along)
    return tuple(jnp.split(lax.all_gather(both, axis, axis=dim, tiled=True), ends, axis=along))


def gather_in_order(x, axes, turns):
    parts = x
    for k in turns:
        parts = lax.all_gather(parts, axes[k])
    done = turns[::-1]
    back = [done.index(k) for k in range(len(axes))]
    parts = parts.transpose(*back, *range(len(axes), parts.ndim))
    return parts.reshape(-1, *x.shape)


def whole_of(x, axes, turns, dim):
    return in_order(gather_in_order(x, axes, turns), dim)


def of_everyone(x, axis):
    return sent_to_all(x, axis).sum(axis=0)


def together(arrays, axis):
    ends = [0]
    for a in arrays:
        ends.append(ends[-1] + a.size)
    so_far = of_everyone(jnp.concatenate([a.ravel() for a in arrays]), axis)
    return tuple((so_far[b:e].reshape(a.shape) for a, b, e in zip(arrays, ends, ends[1:])))


def add_pair(left, pieces):
    return (
        jnp.dot(left, pieces[0], preferred_element_type=jnp.float32),
        jnp.dot(left, pieces[1], preferred_element_type=jnp.float32),
    )


def on_device(
    tokens,
    norm_first,
    norm_mix,
    norm_second,
    gate_weight,
    up_weight,
    down_weight,
    gate_scale,
    up_scale,
    down_scale,
    u_weight,
    v_weight,
    u_scale,
    v_scale,
    ln_gain,
    ln_bias,
    spatial_weight,
    spatial_bias,
    out_weight,
    out_scale,
):
    wide_scales = rows_first((down_scale, out_scale), FS, (0, 0))
    gate_low = gate_weight.astype(jnp.bfloat16)
    up_low = up_weight.astype(jnp.bfloat16)
    down_low = down_weight.astype(jnp.bfloat16)
    count = tokens.shape[0]

    def full_norm(rows, gain):
        whole = gather_directly(rows, "tp", 1)
        values = whole.astype(jnp.float32)
        factor = lax.rsqrt(jnp.mean(values * values, axis=1, keepdims=True) + EPS)
        return (values * factor * gain).astype(jnp.bfloat16)

    def spread_sum(term):
        return sum_at_owner(term.astype(jnp.bfloat16), "tp", 1)

    gate_all, up_all = sent_together((gate_low, up_low), FS, 0, 1)

    def hidden_units(normed):
        gate = jnp.dot(normed, gate_all, preferred_element_type=jnp.float32) * gate_scale
        up_part = jnp.dot(normed, up_all, preferred_element_type=jnp.float32) * up_scale
        return (jax.nn.silu(gate) * up_part).astype(jnp.bfloat16)

    first_hidden = hidden_units(full_norm(tokens, norm_first))
    down_all = whole_of(down_low, FS, (0, 1, 2), 1)
    first_term = (
        jnp.dot(first_hidden, down_all, preferred_element_type=jnp.float32) * wide_scales[0]
    )
    first = spread_sum(first_term)
    middle = (tokens.astype(jnp.float32) + 0.5 * first).astype(jnp.bfloat16)
    mix_normed = full_norm(middle, norm_mix)
    u_low = u_weight.astype(jnp.bfloat16)
    v_low = v_weight.astype(jnp.bfloat16)
    u_acc, v_acc = add_pair(mix_normed, sent_together((u_low, v_low), FS, 0, 1))
    u_pre = u_acc * u_scale
    v_act = jax.nn.gelu(v_acc * v_scale, approximate=True)
    totals = together((jnp.sum(v_act, axis=1), jnp.sum(v_act * v_act, axis=1)), "tp")
    v_mean = (totals[0] / BW)[:, None]
    v_var = (totals[1] / BW)[:, None] - v_mean * v_mean
    v_normed = ((v_act - v_mean) * lax.rsqrt(v_var + EPS) * ln_gain + ln_bias).astype(jnp.bfloat16)
    local_groups = spatial_weight.shape[0]
    channels = v_act.shape[1] // local_groups
    blocks = v_normed.reshape(count // SPAN, SPAN, local_groups, channels)
    lower = jnp.tril(jnp.ones((SPAN, SPAN), jnp.bool_))
    masked = jnp.where(lower[None], spatial_weight, jnp.zeros_like(spatial_weight))
    spatial = jnp.einsum("gts,nsgc->ntgc", masked, blocks, preferred_element_type=jnp.float32)
    spatial = spatial + spatial_bias.T[None, :, :, None]
    mixed = (jax.nn.gelu(u_pre, approximate=True) * spatial.reshape(count, v_act.shape[1])).astype(
        jnp.bfloat16
    )
    out_low = out_weight.astype(jnp.bfloat16)
    mix_term = (
        jnp.dot(mixed, gather_directly(out_low, FS, 1), preferred_element_type=jnp.float32)
        * wide_scales[1]
    )
    second = (middle.astype(jnp.float32) + spread_sum(mix_term)).astype(jnp.bfloat16)
    second_hidden = hidden_units(full_norm(second, norm_second))
    last = spread_sum(
        jnp.dot(second_hidden, down_all, preferred_element_type=jnp.float32) * wide_scales[0]
    )
    return (second.astype(jnp.float32) + 0.5 * last).astype(jnp.bfloat16)


def solution(mesh):
    torus = Mesh(
        mesh.devices.reshape(mesh.shape["rep"], 2, 4, 4, mesh.shape["tp"]),
        ("rep", "fs_0", "fs_1", "fs_2", "tp"),
    )
    in_specs = (
        P(REP_FS, "tp"),
        P(),
        P(),
        P(),
        P(FS, "tp"),
        P(FS, "tp"),
        P("tp", FS),
        P("tp"),
        P("tp"),
        P(FS),
        P(FS, "tp"),
        P(FS, "tp"),
        P("tp"),
        P("tp"),
        P("tp"),
        P("tp"),
        P("tp", None, None),
        P("tp", None),
        P("tp", FS),
        P(FS),
    )
    out_specs = P(REP_FS, "tp")
    return jax.shard_map(
        on_device, mesh=torus, in_specs=in_specs, out_specs=out_specs, check_vma=False
    )
```

profile of v0, /device:TPU:1, one launch (start us, length us, event | category | flops | bytes accessed | tf_op | source)
XLA Modules:
  0.0 554.3 jit_solution(2388582558975060697)
XLA Ops:
  6.5 1.1 convert_element_type.123
  7.6 7.5 %all-gather = bf16[2816,64]{0,1:T(8,128)(2,1)S(1)} all-gather(bf16[1408,64]{0,1:T(8,128)(2,1)S(1)} %convert_element_type.123), channel_id=2, replica_groups=mesh['rep'=2,'fs_0'=2,'fs_1'=4,'fs_2'=4,'tp'=2] {'fs_0'}, dimensions={0}, use_global_device_ids=true | all-gather | bytes 540672 | tf_op jit(solution)/shard_map/all_gather | solution.py:67
  16.0 28.1 %all-gather.13.cloned.1.call-done = bf16[8,1408,64]{1,2,0:T(8,128)(2,1)} async-done(((bf16[2,1408,64]{1,2,0:T(8,128)(2,1)}), bf16[8,1408,64]{1,2,0:T(8,128)(2,1)}) %all-gather.13.cloned.1.call-update) | async-done | bytes 1441808 | tf_op jit(solution)/shard_map/all_gather | solution.py:67
  46.6 1.8 broadcast_in_dim.18
  48.4 4.8 all-to-all-start
  53.2 68.0 %all-gather.3 = f32[32,64,2]{1,2,0:T(2,128)S(1)} all-gather(f32[1,64,2]{1,2,0:T(2,128)S(1)} %maximum_bitcast_fusion), channel_id=1, replica_groups=mesh['rep'=2,'fs_0'=2,'fs_1'=4,'fs_2'=4,'tp'=2] {'fs_0','fs_1','fs_2'}, dimensions={0}, use_global_device_ids=true | all-gather | bytes 16896 | tf_op jit(solution)/shard_map/all_gather | solution.py:19
  121.9 2.2 fusion.5
  124.2 5.8 %copy.78 = bf16[2,4,4,1408,64]{3,4,2,1,0:T(8,128)(2,1)} copy(bf16[2,4,4,1408,64]{3,4,0,1,2:T(8,128)(2,1)} %bitcast.99) | data formatting | bytes 11534336 | tf_op jit(solution)/shard_map/transpose | solution.py:70
  130.0 132.8 %all-gather.9.cloned.1.call-done = bf16[2048,2816]{1,0:T(8,128)(2,1)} async-done(((bf16[64,2816]{1,0:T(8,128)(2,1)}), bf16[2048,2816]{1,0:T(8,128)(2,1)}) %all-gather.9.cloned.1.call-update) | async-done | bytes 11534352 | tf_op jit(solution)/shard_map/all_gather | solution.py:61
  262.8 8.7 %fusion.14 = f32[640,1408]{1,0:T(8,128)} fusion(bf16[640,2048]{0,1:T(8,128)(2,1)S(1)} %copy-done.2, bf16[2048,2816]{1,0:T(8,128)(2,1)} %all-gather.9.cloned.1.call-done, f32[1408]{0:T(1024)S(1)} %copy-done.18), kind=kOutput, calls=%fused_computation.26 | convolution fusion | flops 3691888640 | bytes 11998720 | tf_op jit(solution)/shard_map/dot_general | solution.py:137
  271.5 14.9 %multiply_convert_fusion.2 = bf16[640,2048]{1,0:T(8,128)(2,1)S(1)} fusion(bf16[1408,2048]{0,1:T(8,128)(2,1)} %bitcast.97, f32[2048]{0:T(1024)S(1)} %bitcast.107, bf16[640,2048]{0,1:T(8,128)(2,1)} %fusion.5, bf16[2048,2816]{1,0:T(8,128)(2,1)} %all-gather.9.cloned.1.call-done, f32[640,1408]{1,0:T(8,128)} %fusion.14, f32[1408]{0:T(1024)S(1)} %copy-done.19), kind=kOutput, calls=%fused_computation.16 | convolution fusion | flops 7390904320 | bytes 20395520 | tf_op jit(solution)/shard_map/dot_general | solution.py:144
  286.6 25.1 %all_to_all.41 = bf16[2,640,1024]{2,1,0:T(8,128)(2,1)S(1)} all-to-all(bf16[2,640,1024]{2,1,0:T(8,128)(2,1)S(1)} %bitcast.94), channel_id=1, replica_groups=mesh['rep'=2,'fs_0'=2,'fs_1'=4,'fs_2'=4,'tp'=2] {'tp'}, dimensions={0} | all-to-all | bytes 5242880 | tf_op jit(solution)/shard_map/all_to_all | solution.py:51
  314.5 5.8 %all_to_all.42 = bf16[2,640,1024]{1,2,0:T(8,128)(2,1)S(1)} all-to-all(bf16[2,640,1024]{1,2,0:T(8,128)(2,1)S(1)} %broadcast_in_dim.19), channel_id=1, replica_groups=mesh['rep'=2,'fs_0'=2,'fs_1'=4,'fs_2'=4,'tp'=2] {'tp'}, dimensions={0} | all-to-all | bytes 5242880 | tf_op jit(solution)/shard_map/all_to_all | solution.py:29
  321.0 2.2 fusion.3
  323.2 95.5 %all-gather.11.cloned.1.call-done = bf16[2048,1024]{1,0:T(8,128)(2,1)} async-done(((bf16[64,1024]{1,0:T(8,128)(2,1)}), bf16[2048,1024]{1,0:T(8,128)(2,1)}) %all-gather.11.cloned.1.call-update) | async-done | bytes 4194320 | tf_op jit(solution)/shard_map/all_gather | solution.py:61
  418.7 5.4 fusion.90
  424.0 24.0 %all_to_all.43 = f32[2,1,1280]{2,1,0:T(1,128)S(1)} all-to-all(f32[2,1,1280]{2,1,0:T(1,128)S(1)} %broadcast_in_dim.20), channel_id=1, replica_groups=mesh['rep'=2,'fs_0'=2,'fs_1'=4,'fs_2'=4,'tp'=2] {'tp'}, dimensions={0} | all-to-all | bytes 20480 | tf_op jit(solution)/shard_map/all_to_all | solution.py:29
  448.0 1.6 broadcast_in_dim.23
  449.6 7.2 %all-to-all-start.4 = ((bf16[32,512,64]{1,2,0:T(8,128)(2,1)}), bf16[32,512,64]{1,2,0:T(8,128)(2,1)}, u32[]{:S(2)}, u32[]{:S(2)}) async-start(bf16[32,512,64]{1,2,0:T(8,128)(2,1)} %broadcast_in_dim.23), calls=%async_computation.4 | async-start | bytes 4194304 | tf_op jit(solution)/shard_map/all_to_all | solution.py:29
  456.9 1.6 add_convert_fusion.3
  459.1 1.5 copy.85
  460.6 23.1 %all-to-all-done.4 = bf16[32,512,64]{1,2,0:T(8,128)(2,1)} async-done(((bf16[32,512,64]{1,2,0:T(8,128)(2,1)}), bf16[32,512,64]{1,2,0:T(8,128)(2,1)}, u32[]{:S(2)}, u32[]{:S(2)}) %all-to-all-start.4) | async-done | bytes 2097184 | tf_op jit(solution)/shard_map/all_to_all | solution.py:29
  483.7 8.1 %multiply_convert_fusion.1 = bf16[640,2048]{1,0:T(8,128)(2,1)} fusion(bf16[512,2048]{0,1:T(8,128)(2,1)} %bitcast.20, f32[2048]{0:T(1024)S(1)} %bitcast.109, f32[80,8,4,128]{3,2,1,0:T(4,128)} %bitcast.106, bf16[640,2048]{0,1:T(8,128)(2,1)} %fusion.3, bf16[2048,1024]{1,0:T(8,128)(2,1)} %all-gather.11.cloned.1.call-done, f32[512]{0:T(512)S(1)} %copy-done.21), kind=kOutput, calls=%fused_computation.13 | convolution fusion | flops 2690580480 | bytes 10758144 | tf_op jit(solution)/shard_map/dot_general | solution.py:170
  491.9 2.0 copy.109
  493.9 7.6 %all_to_all.44 = bf16[2,640,1024]{2,1,0:T(8,128)(2,1)S(1)} all-to-all(bf16[2,640,1024]{2,1,0:T(8,128)(2,1)S(1)} %bitcast.95), channel_id=1, replica_groups=mesh['rep'=2,'fs_0'=2,'fs_1'=4,'fs_2'=4,'tp'=2] {'tp'}, dimensions={0} | all-to-all | bytes 5242880 | tf_op jit(solution)/shard_map/all_to_all | solution.py:51
  503.5 6.0 %all_to_all.45 = bf16[2,640,1024]{1,2,0:T(8,128)(2,1)S(1)} all-to-all(bf16[2,640,1024]{1,2,0:T(8,128)(2,1)S(1)} %broadcast_in_dim.24), channel_id=1, replica_groups=mesh['rep'=2,'fs_0'=2,'fs_1'=4,'fs_2'=4,'tp'=2] {'tp'}, dimensions={0} | all-to-all | bytes 5242880 | tf_op jit(solution)/shard_map/all_to_all | solution.py:29
  510.8 1.5 copy-done.3
  512.4 8.7 %fusion.17 = f32[640,1408]{1,0:T(8,128)} fusion(bf16[640,2048]{0,1:T(8,128)(2,1)S(1)} %fusion.1, bf16[2048,2816]{1,0:T(8,128)(2,1)} %all-gather.9.cloned.1.call-done, f32[1408]{0:T(1024)S(1)} %copy-done.18), kind=kOutput, calls=%fused_computation.27 | convolution fusion | flops 3691888640 | bytes 11998720 | tf_op jit(solution)/shard_map/dot_general | solution.py:137
  521.1 16.5 %multiply_convert_fusion = bf16[640,2048]{1,0:T(8,128)(2,1)} fusion(bf16[1408,2048]{0,1:T(8,128)(2,1)} %bitcast.98, f32[2048]{0:T(1024)S(1)} %bitcast.108, bf16[640,2048]{0,1:T(8,128)(2,1)} %copy-done.3, bf16[2048,2816]{1,0:T(8,128)(2,1)} %all-gather.9.cloned.1.call-done, f32[640,1408]{1,0:T(8,128)} %fusion.17, f32[1408]{0:T(1024)S(1)} %copy-done.19), kind=kOutput, calls=%fused_computation.10 | convolution fusion | flops 7390904320 | bytes 20395520 | tf_op jit(solution)/shard_map/dot_general | solution.py:176
  537.5 2.0 copy.108
  539.5 5.8 %all_to_all.46 = bf16[2,640,1024]{2,1,0:T(8,128)(2,1)S(1)} all-to-all(bf16[2,640,1024]{2,1,0:T(8,128)(2,1)S(1)} %bitcast.96), channel_id=1, replica_groups=mesh['rep'=2,'fs_0'=2,'fs_1'=4,'fs_2'=4,'tp'=2] {'tp'}, dimensions={0} | all-to-all | bytes 5242880 | tf_op jit(solution)/shard_map/all_to_all | solution.py:51
  546.0 1.6 add_convert_fusion
  (90 shorter events, 12.2 us)
Async XLA Ops:
  6.5 37.6 %copy-start.4 = (f32[64,1408]{1,0:T(8,128)S(1)}, f32[64,1408]{1,0:T(8,128)}, u32[]{:S(2)}) copy-start(f32[64,1408]{1,0:T(8,128)} %param.24) | copy-start | bytes 1081348
  6.5 37.7 %copy-start.5 = (f32[64,1408]{1,0:T(8,128)S(1)}, f32[64,1408]{1,0:T(8,128)}, u32[]{:S(2)}) copy-start(f32[64,1408]{1,0:T(8,128)} %param.25) | copy-start | bytes 1081348
  6.5 37.6 %all-gather.13.cloned.1.call-start = ((), (), s32[]{:S(2)}) async-start(), calls=%async_computation.10 | async-start | bytes 1802240 | tf_op jit(solution)/shard_map/all_gather | solution.py:67
  7.6 37.5 %copy-start.7 = (f32[64,512]{1,0:T(8,128)S(1)}, f32[64,512]{1,0:T(8,128)}, u32[]{:S(2)}) copy-start(f32[64,512]{1,0:T(8,128)} %param.30) | copy-start | bytes 393220
  7.6 37.5 %copy-start.8 = (f32[64,512]{1,0:T(8,128)S(1)}, f32[64,512]{1,0:T(8,128)}, u32[]{:S(2)}) copy-start(f32[64,512]{1,0:T(8,128)} %param.31) | copy-start | bytes 393220
  15.1 30.7 %copy-start = (bf16[640,1024]{1,0:T(8,128)(2,1)S(1)}, bf16[640,1024]{1,0:T(8,128)(2,1)}, u32[]{:S(2)}) copy-start(bf16[640,1024]{1,0:T(8,128)(2,1)} %param.20) | copy-start | bytes 3932164
  15.9 108.3 %all-gather.15.cloned.1.call-start = ((), (), s32[]{:S(2)}) async-start(), calls=%async_computation.11 | async-start | bytes 7208960 | tf_op jit(solution)/shard_map/all_gather | solution.py:67
  44.1 218.6 %all-gather.9.cloned.1.call-start = ((), (), s32[]{:S(2)}) async-start(), calls=%async_computation.8 | async-start | bytes 11894784 | tf_op jit(solution)/shard_map/all_gather | solution.py:61
  45.0 373.6 %all-gather.11.cloned.1.call-start = ((), (), s32[]{:S(2)}) async-start(), calls=%async_computation.9 | async-start | bytes 4325376 | tf_op jit(solution)/shard_map/all_gather | solution.py:61
  48.4 4.8 copy-start.16
  48.4 4.8 copy-start.17
  48.4 72.9 %copy-start.9 = (f32[512,64]{0,1:T(8,128)S(1)}, f32[512,64]{0,1:T(8,128)}, u32[]{:S(2)}) copy-start(f32[512,64]{0,1:T(8,128)} %param.38) | copy-start | bytes 393220
  48.4 72.9 %all-to-all-start = ((bf16[2,640,1024]{1,2,0:T(8,128)(2,1)}), bf16[2,640,1024]{1,2,0:T(8,128)(2,1)S(1)}, u32[]{:S(2)}, u32[]{:S(2)}) async-start(bf16[2,640,1024]{1,2,0:T(8,128)(2,1)} %broadcast_in_dim.18), calls=%async_computation | async-start | bytes 5242880 | tf_op jit(solution)/shard_map/all_to_all | solution.py:29
  53.2 68.8 %copy-start.10 = (f32[2048]{0:T(1024)S(1)}, f32[2048]{0:T(1024)}, u32[]{:S(2)}) copy-start(f32[2048]{0:T(1024)} %param.21) | copy-start | bytes 24580
  124.2 138.6 %copy-start.2 = (bf16[640,2048]{0,1:T(8,128)(2,1)S(1)}, bf16[640,2048]{0,1:T(8,128)(2,1)}, u32[]{:S(2)}) copy-start(bf16[640,2048]{0,1:T(8,128)(2,1)} %fusion.5) | copy-start | bytes 7864324
  124.2 138.6 %copy-start.18 = (f32[1408]{0:T(1024)S(1)}, f32[1408]{0:T(1024)}, u32[]{:S(2)}) copy-start(f32[1408]{0:T(1024)} %param.27) | copy-start | bytes 16900
  130.0 141.5 %copy-start.19 = (f32[1408]{0:T(1024)S(1)}, f32[1408]{0:T(1024)}, u32[]{:S(2)}) copy-start(f32[1408]{0:T(1024)} %param.28) | copy-start | bytes 16900
  311.7 1.3 copy-start.1
  320.3 0.7 copy-start.11
  321.0 97.6 %copy-start.20 = (f32[512]{0:T(512)S(1)}, f32[512]{0:T(512)}, u32[]{:S(2)}) copy-start(f32[512]{0:T(512)} %param.33) | copy-start | bytes 6148
  449.6 7.3 %copy-start.14 = (f32[512]{0:T(512)S(1)}, f32[512]{0:T(512)}, u32[]{:S(2)}) copy-start(f32[512]{0:T(512)} %param.35) | copy-start | bytes 6148
  449.6 7.3 %copy-start.15 = (f32[512]{0:T(512)S(1)}, f32[512]{0:T(512)}, u32[]{:S(2)}) copy-start(f32[512]{0:T(512)} %param.34) | copy-start | bytes 6148
  449.6 34.1 %all-to-all-start.4 = ((bf16[32,512,64]{1,2,0:T(8,128)(2,1)}), bf16[32,512,64]{1,2,0:T(8,128)(2,1)}, u32[]{:S(2)}, u32[]{:S(2)}) async-start(bf16[32,512,64]{1,2,0:T(8,128)(2,1)} %broadcast_in_dim.23), calls=%async_computation.4 | async-start | bytes 4194304 | tf_op jit(solution)/shard_map/all_to_all | solution.py:29
  456.8 1.9 copy-start.6
  456.8 1.9 copy-start.13
  458.7 25.0 %copy-start.21 = (f32[512]{0:T(512)S(1)}, f32[512]{0:T(512)}, u32[]{:S(2)}) copy-start(f32[512]{0:T(512)} %param.32) | copy-start | bytes 6148
  509.5 0.7 copy-start.12
  510.8 1.5 copy-start.3
Sparse Core Ops, SparseCore 0:
  16.1 27.9 all-gather.12
  45.8 61.8 all-gather.14
  109.3 153.4 all-gather.8
  264.3 154.3 all-gather.10
where the time goes:
time: 564 us; the launch traced here: 554 us
  waiting for transfers between devices  280 us (50%)
  blocking collectives  150 us (27%)
  matrix products  62.6 us (11%)
  local copies, waits for them, and re-layouts  21.1 us (4%)
  other arithmetic  15.4 us (3%)
  between operations  13.7 us (2%)
  starting transfers between devices  12.1 us (2%)
    all_gather x2, waiting for transfers between devices, sent_together(): lax.all_gather(both, axis, axis=dim, tiled=True)  228 us
    all_gather x1, blocking collectives, rows_first(): result, at, done = (lax.all_gather(both, axis, axis=0, tiled=True), 0, [])  68 us
    all_to_all x3, blocking collectives, sum_at_owner(): lax.all_to_all(parts, axis, split_axis=0, concat_axis=0, tiled=True)  38.5 us
    all_to_all x3, blocking collectives, sent_to_all(): lax.all_to_all(jnp.broadcast_to(x[None], (size, *x.shape)), axis, 0, 0, t...  35.8 us
    all_gather x2, waiting for transfers between devices, gather_in_order(): parts = lax.all_gather(parts, axes[k])  28.1 us
    all_to_all x2, waiting for transfers between devices, sent_to_all(): lax.all_to_all(jnp.broadcast_to(x[None], (size, *x.shape)), axis, 0, 0, t...  23.1 us
    dot_general x2, matrix products, hidden_units(): jnp.dot(normed, gate_all, preferred_element_type=jnp.float32) * gate_scale  17.4 us
    dot_general x1, matrix products, on_device(): jnp.dot(second_hidden, down_all, preferred_element_type=jnp.float32)  16.5 us
  transfers between devices with their start and end apart: 6, of which 4 were waited for; matrix products, arithmetic and copies ran while one was open for 8% of the time, Pallas kernels for 0%

commit v1 on v0

v1 whole, which is shorter than its diff:
```python
import jax
import jax.numpy as jnp
from jax import lax
from jax.sharding import Mesh
from jax.sharding import PartitionSpec as P

BW = 1024
SPAN = 128
FS = ("fs_0", "fs_1", "fs_2")
REP_FS = ("rep", "fs_0", "fs_1", "fs_2")


EPS = 1e-06


def other_core(x):
    return lax.ppermute(x, "tp", [(0, 1), (1, 0)])


def on_device(
    tokens,
    norm_first,
    norm_mix,
    norm_second,
    gate_weight,
    up_weight,
    down_weight,
    gate_scale,
    up_scale,
    down_scale,
    u_weight,
    v_weight,
    u_scale,
    v_scale,
    ln_gain,
    ln_bias,
    spatial_weight,
    spatial_bias,
    out_weight,
    out_scale,
):
    count, half = tokens.shape
    units = gate_weight.shape[1]
    chans = u_weight.shape[1]
    first_core = lax.axis_index("tp") == 0

    low = jnp.bfloat16
    gate_low = (gate_weight * gate_scale).astype(low)
    up_low = (up_weight * up_scale).astype(low)
    down_low = (down_weight * down_scale).T.astype(low)
    u_low = (u_weight * u_scale).astype(low)
    v_low = (v_weight * v_scale).astype(low)
    out_low = (out_weight * out_scale).T.astype(low)
    pad = jnp.zeros((gate_low.shape[0], 3 * chans - units), low)
    mine = jnp.where(
        lax.axis_index("rep") == 0,
        jnp.concatenate([gate_low, down_low, pad], axis=1),
        jnp.concatenate([up_low, u_low, v_low, out_low], axis=1),
    )
    both = lax.all_gather(mine, REP_FS, axis=0, tiled=True)
    both = both.reshape(2, -1, both.shape[1])
    gate_all = both[0, :, :units]
    down_all = both[0, :, units : 2 * units]
    up_all = both[1, :, :units]
    u_all = both[1, :, units : units + chans]
    v_all = both[1, :, units + chans : units + 2 * chans]
    out_all = both[1, :, units + 2 * chans :]

    def full_norm(rows, gain):
        other = other_core(rows)
        whole = jnp.concatenate(
            [jnp.where(first_core, rows, other), jnp.where(first_core, other, rows)], axis=1
        )
        values = whole.astype(jnp.float32)
        factor = lax.rsqrt(jnp.mean(values * values, axis=1, keepdims=True) + EPS)
        return (values * factor * gain).astype(low)

    def spread_sum(term):
        term = term.astype(low)
        left, right = term[:, :half], term[:, half:]
        arrived = other_core(jnp.where(first_core, right, left))
        kept = jnp.where(first_core, left, right)
        return kept.astype(jnp.float32) + arrived.astype(jnp.float32)

    def times_rows(left, rows):
        return lax.dot_general(
            left, rows, (((1,), (1,)), ((), ())), preferred_element_type=jnp.float32
        )

    def feed_forward(normed):
        gate = jnp.dot(normed, gate_all, preferred_element_type=jnp.float32)
        up_part = jnp.dot(normed, up_all, preferred_element_type=jnp.float32)
        hidden = (jax.nn.silu(gate) * up_part).astype(low)
        return spread_sum(times_rows(hidden, down_all))

    first = feed_forward(full_norm(tokens, norm_first))
    middle = (tokens.astype(jnp.float32) + 0.5 * first).astype(low)
    mix_normed = full_norm(middle, norm_mix)
    u_pre = jnp.dot(mix_normed, u_all, preferred_element_type=jnp.float32)
    v_act = jax.nn.gelu(
        jnp.dot(mix_normed, v_all, preferred_element_type=jnp.float32), approximate=True
    )
    sums = jnp.stack([jnp.sum(v_act, axis=1), jnp.sum(v_act * v_act, axis=1)])
    totals = sums + other_core(sums)
    v_mean = (totals[0] / BW)[:, None]
    v_var = (totals[1] / BW)[:, None] - v_mean * v_mean
    v_normed = ((v_act - v_mean) * lax.rsqrt(v_var + EPS) * ln_gain + ln_bias).astype(low)
    local_groups = spatial_weight.shape[0]
    channels = chans // local_groups
    blocks = v_normed.reshape(count // SPAN, SPAN, local_groups, channels)
    lower = jnp.tril(jnp.ones((SPAN, SPAN), jnp.bool_))
    masked = jnp.where(lower[None], spatial_weight, jnp.zeros_like(spatial_weight))
    spatial = jnp.einsum("gts,nsgc->ntgc", masked, blocks, preferred_element_type=jnp.float32)
    spatial = spatial + spatial_bias.T[None, :, :, None]
    mixed = (jax.nn.gelu(u_pre, approximate=True) * spatial.reshape(count, chans)).astype(low)
    second = (middle.astype(jnp.float32) + spread_sum(times_rows(mixed, out_all))).astype(low)
    last = feed_forward(full_norm(second, norm_second))
    return (second.astype(jnp.float32) + 0.5 * last).astype(low)


def solution(mesh):
    torus = Mesh(
        mesh.devices.reshape(mesh.shape["rep"], 2, 4, 4, mesh.shape["tp"]),
        ("rep", "fs_0", "fs_1", "fs_2", "tp"),
    )
    in_specs = (
        P(REP_FS, "tp"),
        P(),
        P(),
        P(),
        P(FS, "tp"),
        P(FS, "tp"),
        P("tp", FS),
        P("tp"),
        P("tp"),
        P(FS),
        P(FS, "tp"),
        P(FS, "tp"),
        P("tp"),
        P("tp"),
        P("tp"),
        P("tp"),
        P("tp", None, None),
        P("tp", None),
        P("tp", FS),
        P(FS),
    )
    out_specs = P(REP_FS, "tp")
    return jax.shard_map(
        on_device, mesh=torus, in_specs=in_specs, out_specs=out_specs, check_vma=False
    )
```

time: 564 us -> 243 us (0.43); the launches traced: 554 us -> 243 us
  blocking collectives: 150 us -> 0 us
  waiting for transfers between devices: 280 us -> 141 us
  local copies, waits for them, and re-layouts: 21.1 us -> 2.58 us
  starting transfers between devices: 12.1 us -> 4.96 us
    all_gather x4 -> x1, waiting for transfers between devices: 256 us -> 124 us  [on_device(): both = lax.all_gather(mine, REP_FS, axis=0, tiled=True)]
    all_gather x2 -> x0, blocking collectives: 75.5 us -> none  [the longest x1 68 us: rows_first(): result, at, done = (lax.all_gather(both, axis, axis=0, tiled=True), 0, [])]
    all_to_all x6 -> x0, blocking collectives: 74.3 us -> none  [the longest x3 38.5 us: sum_at_owner(): lax.all_to_all(parts, axis, split_axis=0, concat_axis=0, tiled=True)]
    all_to_all x2 -> x0, waiting for transfers between devices: 23.1 us -> none  [sent_to_all(): lax.all_to_all(jnp.broadcast_to(x[None], (size, *x.shape)), axis, 0, 0, t...]
    ppermute x0 -> x7, waiting for transfers between devices: none -> 16.7 us  [other_core(): return lax.ppermute(x, 'tp', [(0, 1), (1, 0)])]
    all_to_all x2 -> x0, starting transfers between devices: 12 us -> none  [sent_to_all(): lax.all_to_all(jnp.broadcast_to(x[None], (size, *x.shape)), axis, 0, 0, t...]
    select_n x0 -> x7, other arithmetic: none -> 7.6 us  [the longest x3 4.13 us: spread_sum(): arrived = other_core(jnp.where(first_core, right, left))]
    transpose x1 -> x0, local copies, waits for them, and re-layouts: 5.8 us -> none  [gather_in_order(): parts = parts.transpose(*back, *range(len(axes), parts.ndim))]
  transfers between devices with their start and end apart: 6 -> 8, of which waited for: 4 -> 8; matrix products, arithmetic and copies ran while one was open for 8% -> 1% of each run, Pallas kernels for 0% -> 0%
where the time goes in v1:
time: 243 us
  waiting for transfers between devices  141 us (58%)
  matrix products  60.2 us (25%)
  other arithmetic  20.5 us (8%)
  between operations  13.7 us (6%)
  starting transfers between devices  4.96 us (2%)
  local copies, waits for them, and re-layouts  2.58 us (1%)
    all_gather x1, waiting for transfers between devices, on_device(): both = lax.all_gather(mine, REP_FS, axis=0, tiled=True)  124 us
    dot_general x3, matrix products, times_rows(): lax.dot_general(left, rows, (((1,), (1,)), ((), ())), preferred_element_t...  38.4 us
    dot_general x2, matrix products, feed_forward(): gate = jnp.dot(normed, gate_all, preferred_element_type=jnp.float32)  17.6 us
    ppermute x7, waiting for transfers between devices, other_core(): return lax.ppermute(x, 'tp', [(0, 1), (1, 0)])  16.7 us
    ppermute x7, starting transfers between devices, other_core(): return lax.ppermute(x, 'tp', [(0, 1), (1, 0)])  4.95 us
  transfers between devices with their start and end apart: 8, of which 8 were waited for; matrix products, arithmetic and copies ran while one was open for 1% of the time, Pallas kernels for 0%

profile of v1, /device:TPU:1, one launch (start us, length us, event | category | flops | bytes accessed | tf_op | source)
XLA Modules:
  0.0 243.1 jit_solution(3180646621840350254)
XLA Ops:
  6.6 1.1 fusion.51
  7.6 1.1 fusion.47
  8.7 1.0 multiply_convert_fusion.4
  9.7 1.2 multiply_convert_fusion
  10.9 0.9 maximum_select_fusion
  11.8 1.5 collective-permute-start
  13.3 2.8 %collective-permute-done = bf16[640,1024]{1,0:T(8,128)(2,1)} collective-permute-done((bf16[640,1024]{1,0:T(8,128)(2,1)S(1)}, bf16[640,1024]{1,0:T(8,128)(2,1)}, u32[]{:S(2)}, u32[]{:S(2)}) %collective-permute-start) | collective-permute-done | bytes 1310752 | tf_op jit(solution)/shard_map/ppermute | solution.py:17
  16.1 1.9 broadcast_select_fusion.8
  18.0 0.6 fusion
  18.6 124.4 %all-gather.2.cloned.1.call-done = bf16[4096,2944]{1,0:T(8,128)(2,1)} async-done(((bf16[64,2944]{1,0:T(8,128)(2,1)}), bf16[4096,2944]{1,0:T(8,128)(2,1)}) %all-gather.2.cloned.1.call-update) | async-done | bytes 24117264 | tf_op jit(solution)/shard_map/all_gather | solution.py:60
  143.1 8.8 %fusion.10 = f32[640,1408]{1,0:T(8,128)} fusion(bf16[2,2048,2944]{2,1,0:T(8,128)(2,1)} %bitcast.68, f32[2048]{0:T(1024)S(1)} %copy-done.14, f32[640]{0:T(1024)S(1)} %add_rsqrt_fusion.3, bf16[640,1024]{1,0:T(8,128)(2,1)S(1)} %get-tuple-element.14, bf16[640,1024]{1,0:T(8,128)(2,1)S(1)} %get-tuple-element.13), kind=kOutput, calls=%fused_computation.19 | convolution fusion | flops 3700162560 | bytes 12003840 | tf_op jit(solution)/shard_map/dot_general | solution.py:91
  151.9 14.5 %fusion.19 = bf16[640,2048]{1,0:T(8,128)(2,1)S(1)} fusion(bf16[2,2048,2944]{2,1,0:T(8,128)(2,1)} %bitcast.69, f32[640,1408]{1,0:T(8,128)} %fusion.10, f32[2048]{0:T(1024)S(1)} %copy-done.14, f32[640]{0:T(1024)S(1)} %add_rsqrt_fusion.3, bf16[640,1024]{1,0:T(8,128)(2,1)} %copy-done.6, bf16[640,1024]{1,0:T(8,128)(2,1)} %copy-done.5), kind=kOutput, calls=%fused_computation.28 | convolution fusion | flops 7397867520 | bytes 20392448 | tf_op jit(solution)/shard_map/dot_general | solution.py:86
  166.6 1.1 collective-permute-start.1
  168.0 2.4 collective-permute-done.1
  170.4 2.9 %add_convert_fusion.2 = bf16[640,1024]{1,0:T(8,128)(2,1)S(1)} fusion(bf16[640,1024]{1,0:T(8,128)(2,1)S(1)} %collective-permute-done.1, bf16[640,1024]{1,0:T(8,128)(2,1)S(1)} %copy-done.9, pred[]{:T(512)S(6)} %eq.6, bf16[640,2048]{1,0:T(8,128)(2,1)} %copy-done.2), kind=kLoop, calls=%fused_computation.36 | loop fusion | flops 5242880 | bytes 6553601 | tf_op jit(solution)/shard_map/convert_element_type | solution.py:97
  173.7 2.7 %collective-permute-done.2 = bf16[640,1024]{1,0:T(8,128)(2,1)S(1)} collective-permute-done((bf16[640,1024]{1,0:T(8,128)(2,1)S(1)}, bf16[640,1024]{1,0:T(8,128)(2,1)S(1)}, u32[]{:S(2)}, u32[]{:S(2)}) %collective-permute-start.2) | collective-permute-done | bytes 1310752 | tf_op jit(solution)/shard_map/ppermute | solution.py:17
  176.8 0.6 fusion.3
  177.5 3.8 %fusion.72 = (f32[640]{0:T(1024)S(1)}, f32[640]{0:T(1024)S(1)}, f32[640,512]{1,0:T(8,128)S(1)}) fusion(bf16[2,2048,2944]{2,1,0:T(8,128)(2,1)} %bitcast.70, f32[2048]{0:T(1024)S(1)} %copy-done.15, f32[640]{0:T(1024)S(1)} %add_rsqrt_fusion.2, bf16[640,1024]{1,0:T(8,128)(2,1)S(1)} %get-tuple-element.12, bf16[640,1024]{1,0:T(8,128)(2,1)S(1)} %get-tuple-element.11), kind=kOutput, calls=%fused_computation.111 | convolution fusion | flops 1354955520 | bytes 6045184 | tf_op jit(solution)/shard_map/dot_general | solution.py:101
  181.8 0.8 collective-permute-done.3
  183.6 1.5 copy.27
  185.1 8.1 %convolution_convert_fusion = bf16[640,2048]{1,0:T(8,128)(2,1)} fusion(bf16[2,2048,2944]{2,1,0:T(8,128)(2,1)} %bitcast.71, f32[80,8,4,128]{3,2,1,0:T(4,128)} %bitcast.66, f32[2048]{0:T(1024)S(1)} %copy-done.15, f32[640]{0:T(1024)S(1)} %add_rsqrt_fusion.2, bf16[640,1024]{1,0:T(8,128)(2,1)} %copy-done.4, bf16[640,1024]{1,0:T(8,128)(2,1)} %copy-done.3), kind=kOutput, calls=%fused_computation.30 | convolution fusion | flops 2698117120 | bytes 10758656 | tf_op jit(solution)/shard_map/dot_general | solution.py:86
  193.2 2.0 broadcast_select_fusion.3
  195.6 2.7 %collective-permute-done.4 = bf16[640,1024]{1,0:T(8,128)(2,1)S(1)} collective-permute-done((bf16[640,1024]{1,0:T(8,128)(2,1)S(1)}, bf16[640,1024]{1,0:T(8,128)(2,1)S(1)}, u32[]{:S(2)}, u32[]{:S(2)}) %collective-permute-start.4) | collective-permute-done | bytes 1310752 | tf_op jit(solution)/shard_map/ppermute | solution.py:17
  198.3 1.2 add_convert_fusion.1
  199.5 0.6 collective-permute-start.5
  200.2 2.7 %collective-permute-done.5 = bf16[640,1024]{1,0:T(8,128)(2,1)S(1)} collective-permute-done((bf16[640,1024]{1,0:T(8,128)(2,1)S(1)}, bf16[640,1024]{1,0:T(8,128)(2,1)S(1)}, u32[]{:S(2)}, u32[]{:S(2)}) %collective-permute-start.5) | collective-permute-done | bytes 1310752 | tf_op jit(solution)/shard_map/ppermute | solution.py:17
  203.2 0.6 fusion.6
  204.3 8.8 %fusion.9 = f32[640,1408]{1,0:T(8,128)} fusion(bf16[2,2048,2944]{2,1,0:T(8,128)(2,1)} %bitcast.72, f32[2048]{0:T(1024)S(1)} %copy-done.16, f32[640]{0:T(1024)S(1)} %add_rsqrt_fusion, bf16[640,1024]{1,0:T(8,128)(2,1)S(1)} %get-tuple-element.10, bf16[640,1024]{1,0:T(8,128)(2,1)S(1)} %get-tuple-element.9), kind=kOutput, calls=%fused_computation.18 | convolution fusion | flops 3700162560 | bytes 12003840 | tf_op jit(solution)/shard_map/dot_general | solution.py:91
  213.1 15.7 %fusion.20 = bf16[640,2048]{1,0:T(8,128)(2,1)} fusion(bf16[2,2048,2944]{2,1,0:T(8,128)(2,1)} %bitcast.73, f32[640,1408]{1,0:T(8,128)} %fusion.9, f32[2048]{0:T(1024)S(1)} %copy-done.16, f32[640]{0:T(1024)S(1)} %add_rsqrt_fusion, bf16[640,1024]{1,0:T(8,128)(2,1)} %copy-done.7, bf16[640,1024]{1,0:T(8,128)(2,1)S(1)} %get-tuple-element.9), kind=kOutput, calls=%fused_computation.29 | convolution fusion | flops 7397867520 | bytes 20392448 | tf_op jit(solution)/shard_map/dot_general | solution.py:86
  228.8 2.0 broadcast_select_fusion
  231.2 2.7 %collective-permute-done.6 = bf16[640,1024]{1,0:T(8,128)(2,1)S(1)} collective-permute-done((bf16[640,1024]{1,0:T(8,128)(2,1)S(1)}, bf16[640,1024]{1,0:T(8,128)(2,1)S(1)}, u32[]{:S(2)}, u32[]{:S(2)}) %collective-permute-start.6) | collective-permute-done | bytes 1310752 | tf_op jit(solution)/shard_map/ppermute | solution.py:17
  233.9 2.3 add_convert_fusion
  (58 shorter events, 4.4 us)
Async XLA Ops:
  6.5 5.3 %copy-start.8 = (bf16[640,1024]{1,0:T(8,128)(2,1)S(1)}, bf16[640,1024]{1,0:T(8,128)(2,1)}, u32[]{:S(2)}) copy-start(bf16[640,1024]{1,0:T(8,128)(2,1)} %param.20) | copy-start | bytes 3932164
  6.5 136.5 %all-gather.2.cloned.1.call-start = ((), (), s32[]{:S(2)}) async-start(), calls=%async_computation | async-start | bytes 24494080 | tf_op jit(solution)/shard_map/all_gather | solution.py:60
  11.8 4.3 %collective-permute-start = (bf16[640,1024]{1,0:T(8,128)(2,1)S(1)}, bf16[640,1024]{1,0:T(8,128)(2,1)}, u32[]{:S(2)}, u32[]{:S(2)}) collective-permute-start(bf16[640,1024]{1,0:T(8,128)(2,1)S(1)} %copy-done.8), channel_id=1, source_target_pairs={{0,1},{1,0},{2,3},{3,2},{4,5},{5,4},{6,7},{7,6},{8,9},{9,8},{10,11... | collective-permute-start | bytes 3932168 | tf_op jit(solution)/shard_map/ppermute | solution.py:17
  18.0 125.1 %copy-start.5 = (bf16[640,1024]{1,0:T(8,128)(2,1)}, bf16[640,1024]{1,0:T(8,128)(2,1)S(1)}, u32[]{:S(2)}) copy-start(bf16[640,1024]{1,0:T(8,128)(2,1)S(1)} %get-tuple-element.13) | copy-start | bytes 3932164
  18.0 125.1 %copy-start.6 = (bf16[640,1024]{1,0:T(8,128)(2,1)}, bf16[640,1024]{1,0:T(8,128)(2,1)S(1)}, u32[]{:S(2)}) copy-start(bf16[640,1024]{1,0:T(8,128)(2,1)S(1)} %get-tuple-element.14) | copy-start | bytes 3932164
  18.0 125.1 %copy-start.14 = (f32[2048]{0:T(1024)S(1)}, f32[2048]{0:T(1024)}, u32[]{:S(2)}) copy-start(f32[2048]{0:T(1024)} %param.21) | copy-start | bytes 24580
  166.4 1.5 copy-start.2
  166.4 3.9 %copy-start.9 = (bf16[640,1024]{1,0:T(8,128)(2,1)S(1)}, bf16[640,1024]{1,0:T(8,128)(2,1)}, u32[]{:S(2)}) copy-start(bf16[640,1024]{1,0:T(8,128)(2,1)} %param.20) | copy-start | bytes 3932164
  166.6 3.8 %collective-permute-start.1 = (bf16[640,1024]{1,0:T(8,128)(2,1)S(1)}, bf16[640,1024]{1,0:T(8,128)(2,1)S(1)}, u32[]{:S(2)}, u32[]{:S(2)}) collective-permute-start(bf16[640,1024]{1,0:T(8,128)(2,1)S(1)} %broadcast_select_fusion.6), channel_id=1, source_target_pairs={{0,1},{1,0},{2,3},{3,2},{4,5},{5,4},{6,7},{7,6},{8,9},{9,8},{10,11... | collective-permute-start | bytes 3932168 | tf_op jit(solution)/shard_map/ppermute | solution.py:17
  173.3 3.1 %collective-permute-start.2 = (bf16[640,1024]{1,0:T(8,128)(2,1)S(1)}, bf16[640,1024]{1,0:T(8,128)(2,1)S(1)}, u32[]{:S(2)}, u32[]{:S(2)}) collective-permute-start(bf16[640,1024]{1,0:T(8,128)(2,1)S(1)} %add_convert_fusion.2), channel_id=1, source_target_pairs={{0,1},{1,0},{2,3},{3,2},{4,5},{5,4},{6,7},{7,6},{8,9},{9,8},{10,11... | collective-permute-start | bytes 3932168 | tf_op jit(solution)/shard_map/ppermute | solution.py:17
  176.7 4.6 %copy-start.3 = (bf16[640,1024]{1,0:T(8,128)(2,1)}, bf16[640,1024]{1,0:T(8,128)(2,1)S(1)}, u32[]{:S(2)}) copy-start(bf16[640,1024]{1,0:T(8,128)(2,1)S(1)} %get-tuple-element.11) | copy-start | bytes 3932164
  176.7 4.6 %copy-start.4 = (bf16[640,1024]{1,0:T(8,128)(2,1)}, bf16[640,1024]{1,0:T(8,128)(2,1)S(1)}, u32[]{:S(2)}) copy-start(bf16[640,1024]{1,0:T(8,128)(2,1)S(1)} %get-tuple-element.12) | copy-start | bytes 3932164
  176.8 0.7 copy-start.15
  177.5 5.2 %copy-start.12 = (f32[512]{0:T(512)S(1)}, f32[512]{0:T(512)}, u32[]{:S(2)}) copy-start(f32[512]{0:T(512)} %param.35) | copy-start | bytes 6148
  177.5 5.2 %copy-start.13 = (f32[512]{0:T(512)S(1)}, f32[512]{0:T(512)}, u32[]{:S(2)}) copy-start(f32[512]{0:T(512)} %param.34) | copy-start | bytes 6148
  181.3 1.9 copy-start.10
  181.3 1.8 copy-start.11
  181.4 1.3 collective-permute-start.3
  193.2 5.1 %copy-start.1 = (bf16[640,2048]{1,0:T(8,128)(2,1)S(1)}, bf16[640,2048]{1,0:T(8,128)(2,1)}, u32[]{:S(2)}) copy-start(bf16[640,2048]{1,0:T(8,128)(2,1)} %convolution_convert_fusion) | copy-start | bytes 7864324
  195.2 3.1 %collective-permute-start.4 = (bf16[640,1024]{1,0:T(8,128)(2,1)S(1)}, bf16[640,1024]{1,0:T(8,128)(2,1)S(1)}, u32[]{:S(2)}, u32[]{:S(2)}) collective-permute-start(bf16[640,1024]{1,0:T(8,128)(2,1)S(1)} %broadcast_select_fusion.3), channel_id=1, source_target_pairs={{0,1},{1,0},{2,3},{3,2},{4,5},{5,4},{6,7},{7,6},{8,9},{9,8},{10,11... | collective-permute-start | bytes 3932168 | tf_op jit(solution)/shard_map/ppermute | solution.py:17
  199.5 3.3 %collective-permute-start.5 = (bf16[640,1024]{1,0:T(8,128)(2,1)S(1)}, bf16[640,1024]{1,0:T(8,128)(2,1)S(1)}, u32[]{:S(2)}, u32[]{:S(2)}) collective-permute-start(bf16[640,1024]{1,0:T(8,128)(2,1)S(1)} %add_convert_fusion.1), channel_id=1, source_target_pairs={{0,1},{1,0},{2,3},{3,2},{4,5},{5,4},{6,7},{7,6},{8,9},{9,8},{10,11... | collective-permute-start | bytes 3932168 | tf_op jit(solution)/shard_map/ppermute | solution.py:17
  203.2 1.1 copy-start.7
  203.2 1.0 copy-start.16
  228.8 5.1 %copy-start = (bf16[640,2048]{1,0:T(8,128)(2,1)S(1)}, bf16[640,2048]{1,0:T(8,128)(2,1)}, u32[]{:S(2)}) copy-start(bf16[640,2048]{1,0:T(8,128)(2,1)} %fusion.20) | copy-start | bytes 7864324
  230.8 3.1 %collective-permute-start.6 = (bf16[640,1024]{1,0:T(8,128)(2,1)S(1)}, bf16[640,1024]{1,0:T(8,128)(2,1)S(1)}, u32[]{:S(2)}, u32[]{:S(2)}) collective-permute-start(bf16[640,1024]{1,0:T(8,128)(2,1)S(1)} %broadcast_select_fusion), channel_id=1, source_target_pairs={{0,1},{1,0},{2,3},{3,2},{4,5},{5,4},{6,7},{7,6},{8,9},{9,8},{10,11... | collective-permute-start | bytes 3932168 | tf_op jit(solution)/shard_map/ppermute | solution.py:17
Sparse Core Ops, SparseCore 0:
  12.0 131.0 all-gather.1

commit v2 on v1

v2 whole, which is shorter than its diff:
```python
import functools

import jax
import jax.numpy as jnp
from jax import lax
from jax.experimental import pallas as pl
from jax.experimental.pallas import tpu as pltpu
from jax.sharding import Mesh
from jax.sharding import PartitionSpec as P

BW = 1024
SPAN = 128
FS = ("fs_0", "fs_1", "fs_2")
REP_FS = ("rep", "fs_0", "fs_1", "fs_2")
LANES = 128
WIDE = 256

EPS = 1e-06


def other_core(x):
    return lax.ppermute(x, "tp", [(0, 1), (1, 0)])


def normed_rows(values, gain):
    factor = lax.rsqrt(jnp.mean(values * values, axis=1, keepdims=True) + EPS)
    return (values * factor * gain).astype(jnp.bfloat16)


def dot(left, right):
    return jnp.dot(left, right, preferred_element_type=jnp.float32)


def dot_rows(left, rows):
    return lax.dot_general(
        left, rows, (((1,), (1,)), ((), ())), preferred_element_type=jnp.float32
    )


def gelu(a):
    return 0.5 * a * (1.0 + jnp.tanh(0.7978845608028654 * (a + 0.044715 * a * a * a)))


def hidden_tile(normed, gate, up):
    both = dot(normed, jnp.concatenate([gate, up], axis=1))
    gate_part, up_part = both[:, :LANES], both[:, LANES:]
    return (gate_part / (1.0 + jnp.exp(-gate_part)) * up_part).astype(jnp.bfloat16)


def spec(block, index):
    return pl.BlockSpec(block, index)


def whole(shape):
    return pl.BlockSpec(shape, lambda *_: (0,) * len(shape))


def params(steps):
    return pltpu.CompilerParams(
        dimension_semantics=("arbitrary",) * steps, vmem_limit_bytes=60 * 1024 * 1024
    )


def cost(flops, moved, special):
    return pl.CostEstimate(flops=flops, bytes_accessed=moved, transcendentals=special)


def first_kernel(tiles, core, own, other, gain, gate, up, down, term, normed, hidden):
    step = pl.program_id(0)

    @pl.when(step == 0)
    def _():
        left = jnp.where(core[0] == 0, own[...], other[...])
        right = jnp.where(core[0] == 0, other[...], own[...])
        values = jnp.concatenate([left, right], axis=1).astype(jnp.float32)
        normed[...] = normed_rows(values, gain[...])

    @pl.when(step < tiles)
    def _():
        hidden[step] = hidden_tile(normed[...], gate[0], up[0])

    @pl.when(step >= tiles)
    def _():
        units = jnp.concatenate([hidden[k] for k in range(tiles)], axis=1)
        term[...] = dot_rows(units, down[0]).astype(jnp.bfloat16)


def first_pass(core, own, other, gain, both):
    count, half = own.shape
    width = 2 * half
    units = both.shape[2] // 2 // LANES * LANES
    tiles, outs = units // LANES, width // WIDE
    shift = both.shape[2] // LANES - tiles
    return pl.pallas_call(
        functools.partial(first_kernel, tiles),
        out_shape=jax.ShapeDtypeStruct((count, width), jnp.bfloat16),
        grid_spec=pltpu.PrefetchScalarGridSpec(
            num_scalar_prefetch=1,
            grid=(tiles + outs,),
            in_specs=[
                whole((count, half)),
                whole((count, half)),
                whole((1, width)),
                spec((1, width, LANES), lambda j, c: (0, 0, jnp.minimum(j, tiles - 1))),
                spec((1, width, LANES), lambda j, c: (1, 0, shift + jnp.minimum(j, tiles - 1))),
                spec((1, WIDE, units), lambda j, c: (0, jnp.maximum(j - tiles, 0), 1)),
            ],
            out_specs=spec((count, WIDE), lambda j, c: (0, jnp.maximum(j - tiles, 0))),
            scratch_shapes=[
                pltpu.VMEM((count, width), jnp.bfloat16),
                pltpu.VMEM((tiles, count, LANES), jnp.bfloat16),
            ],
        ),
        compiler_params=params(1),
        cost_estimate=cost(6 * count * width * units, 6 * width * units, count * units),
        name="first_pass",
    )(core, own, other, gain, both, both, both)


def second_kernel(
    tiles, sent, core, middle, term, far, gain, gate, up, down, send, keep, base, normed, hidden
):
    step = pl.program_id(0)

    @pl.when(step == 0)
    def _():
        values = middle[...].astype(jnp.float32) + (
            term[...].astype(jnp.float32) + far[...].astype(jnp.float32)
        )
        second = values.astype(jnp.bfloat16)
        half = second.shape[1] // 2
        base[...] = jnp.where(core[0] == 0, second[:, :half], second[:, half:])
        normed[...] = normed_rows(second.astype(jnp.float32), gain[...])

    @pl.when(step < tiles)
    def _():
        hidden[step] = hidden_tile(normed[...], gate[0], up[0])

    @pl.when(step >= tiles)
    def _():
        units = jnp.concatenate([hidden[k] for k in range(tiles)], axis=1)
        part = dot_rows(units, down[0]).astype(jnp.bfloat16)

        @pl.when(step < tiles + sent)
        def _():
            send[...] = part

        @pl.when(step >= tiles + sent)
        def _():
            keep[...] = part


def second_pass(core, middle, term, far, gain, both):
    count, width = middle.shape
    half = width // 2
    units = both.shape[2] // 2 // LANES * LANES
    tiles, outs = units // LANES, width // WIDE
    sent = outs // 2
    shift = both.shape[2] // LANES - tiles

    def rows_of(j, c):
        n = jnp.maximum(j - tiles, 0)
        return jnp.where(n < sent, n + (1 - c[0]) * sent, n - sent + c[0] * sent)

    return pl.pallas_call(
        functools.partial(second_kernel, tiles, sent),
        out_shape=[jax.ShapeDtypeStruct((count, half), jnp.bfloat16)] * 3,
        grid_spec=pltpu.PrefetchScalarGridSpec(
            num_scalar_prefetch=1,
            grid=(tiles + outs,),
            in_specs=[
                whole((count, width)),
                whole((count, width)),
                whole((count, width)),
                whole((1, width)),
                spec((1, width, LANES), lambda j, c: (0, 0, jnp.minimum(j, tiles - 1))),
                spec((1, width, LANES), lambda j, c: (1, 0, shift + jnp.minimum(j, tiles - 1))),
                spec((1, WIDE, units), lambda j, c: (0, rows_of(j, c), 1)),
            ],
            out_specs=[
                spec((count, WIDE), lambda j, c: (0, jnp.clip(j - tiles, 0, sent - 1))),
                spec((count, WIDE), lambda j, c: (0, jnp.maximum(j - tiles - sent, 0))),
                whole((count, half)),
            ],
            scratch_shapes=[
                pltpu.VMEM((count, width), jnp.bfloat16),
                pltpu.VMEM((tiles, count, LANES), jnp.bfloat16),
            ],
        ),
        compiler_params=params(1),
        cost_estimate=cost(6 * count * width * units, 6 * width * units, count * units),
        name="second_pass",
    )(core, middle, term, far, gain, both, both, both)


def gates_kernel(core, own, other, term, far, gain, u_rows, v_rows, middle, u_out, v_out, sums):
    left = jnp.where(core[0] == 0, own[...], other[...])
    right = jnp.where(core[0] == 0, other[...], own[...])
    values = jnp.concatenate([left, right], axis=1).astype(jnp.float32)
    values = values + 0.5 * (term[...].astype(jnp.float32) + far[...].astype(jnp.float32))
    mid = values.astype(jnp.bfloat16)
    middle[...] = mid
    normed = normed_rows(mid.astype(jnp.float32), gain[...])
    v_act = gelu(dot(normed, v_rows[0]))
    v_out[...] = v_act
    lane = lax.broadcasted_iota(jnp.int32, sums.shape, 1)
    total = jnp.sum(v_act, axis=1, keepdims=True)
    squares = jnp.sum(v_act * v_act, axis=1, keepdims=True)
    sums[...] = jnp.where(lane == 0, total, squares)
    u_out[...] = gelu(dot(normed, u_rows[0]))


def gates(core, own, other, term, far, gain, both, chans):
    count, half = own.shape
    width = 2 * half
    rows = SPAN

    def block(columns):
        return spec((rows, columns), lambda i, c: (i, 0))

    return pl.pallas_call(
        gates_kernel,
        out_shape=[
            jax.ShapeDtypeStruct((count, width), jnp.bfloat16),
            jax.ShapeDtypeStruct((count, chans), jnp.float32),
            jax.ShapeDtypeStruct((count, chans), jnp.float32),
            jax.ShapeDtypeStruct((count, LANES), jnp.float32),
        ],
        grid_spec=pltpu.PrefetchScalarGridSpec(
            num_scalar_prefetch=1,
            grid=(count // rows,),
            in_specs=[
                block(half),
                block(half),
                block(width),
                block(width),
                whole((1, width)),
                spec((1, width, chans), lambda i, c: (1, 0, 0)),
                spec((1, width, chans), lambda i, c: (1, 0, 1)),
            ],
            out_specs=[block(width), block(chans), block(chans), block(LANES)],
        ),
        compiler_params=params(1),
        cost_estimate=cost(4 * count * width * chans, 4 * width * chans, 2 * count * chans),
        name="gates",
    )(core, own, other, term, far, gain, both, both)


def mix_kernel(u_act, v_act, sums, far, gain, bias, weight, shift, rows, term, masked):
    groups = weight.shape[0]

    @pl.when(pl.program_id(0) == 0)
    def _():
        at = lax.broadcasted_iota(jnp.int32, (SPAN, SPAN), 0)
        source = lax.broadcasted_iota(jnp.int32, (SPAN, SPAN), 1)
        for g in range(groups):
            masked[g] = jnp.where(source <= at, weight[g], jnp.zeros_like(weight[g]))

    totals = (sums[...] + far[...]) / BW
    v_mean = totals[:, 0:1]
    v_var = totals[:, 1:2] - v_mean * v_mean
    v_normed = (v_act[...] - v_mean) * lax.rsqrt(v_var + EPS) * gain[...] + bias[...]
    v_normed = v_normed.astype(jnp.bfloat16)
    wide = v_normed.shape[1] // groups
    spatial = [
        dot(masked[g], v_normed[:, g * wide : (g + 1) * wide]) + shift[:, g : g + 1]
        for g in range(groups)
    ]
    mixed = (u_act[...] * jnp.concatenate(spatial, axis=1)).astype(jnp.bfloat16)
    term[...] = dot_rows(mixed, rows[0]).astype(jnp.bfloat16)


def mix(u_act, v_act, sums, far, gain, bias, weight, shift, both):
    count, chans = u_act.shape
    width = both.shape[1]
    groups = weight.shape[0]

    def block(columns):
        return spec((SPAN, columns), lambda i: (i, 0))

    return pl.pallas_call(
        mix_kernel,
        out_shape=jax.ShapeDtypeStruct((count, width), jnp.bfloat16),
        grid=(count // SPAN,),
        in_specs=[
            block(chans),
            block(chans),
            block(LANES),
            block(LANES),
            whole((1, chans)),
            whole((1, chans)),
            whole((groups, SPAN, SPAN)),
            whole((SPAN, groups)),
            spec((1, width, chans), lambda i: (1, 0, 2)),
        ],
        out_specs=block(width),
        scratch_shapes=[pltpu.VMEM((groups, SPAN, SPAN), jnp.bfloat16)],
        compiler_params=params(1),
        cost_estimate=cost(2 * count * width * chans, 2 * width * chans, count),
        name="mix",
    )(u_act, v_act, sums, far, gain, bias, weight, shift, both)


def on_device(
    tokens,
    norm_first,
    norm_mix,
    norm_second,
    gate_weight,
    up_weight,
    down_weight,
    gate_scale,
    up_scale,
    down_scale,
    u_weight,
    v_weight,
    u_scale,
    v_scale,
    ln_gain,
    ln_bias,
    spatial_weight,
    spatial_bias,
    out_weight,
    out_scale,
):
    units = gate_weight.shape[1]
    chans = u_weight.shape[1]
    core = lax.axis_index("tp").reshape(1).astype(jnp.int32)

    low = jnp.bfloat16
    gate_low = (gate_weight * gate_scale).astype(low)
    up_low = (up_weight * up_scale).astype(low)
    down_low = (down_weight * down_scale).T.astype(low)
    u_low = (u_weight * u_scale).astype(low)
    v_low = (v_weight * v_scale).astype(low)
    out_low = (out_weight * out_scale).T.astype(low)
    pad = jnp.zeros((gate_low.shape[0], 3 * chans - units), low)
    mine = jnp.where(
        lax.axis_index("rep") == 0,
        jnp.concatenate([gate_low, down_low, pad], axis=1),
        jnp.concatenate([u_low, v_low, out_low, up_low], axis=1),
    )
    both = lax.all_gather(mine, REP_FS, axis=0, tiled=True)
    both = both.reshape(2, -1, both.shape[1])

    own, other = tokens, other_core(tokens)
    term = first_pass(core, own, other, norm_first[None], both)
    middle, u_act, v_act, sums = gates(
        core, own, other, term, other_core(term), norm_mix[None], both, chans
    )
    term = mix(
        u_act,
        v_act,
        sums,
        other_core(sums),
        ln_gain[None],
        ln_bias[None],
        spatial_weight,
        spatial_bias.T,
        both,
    )
    send, keep, base = second_pass(core, middle, term, other_core(term), norm_second[None], both)
    last = keep.astype(jnp.float32) + other_core(send).astype(jnp.float32)
    return (base.astype(jnp.float32) + 0.5 * last).astype(low)


def solution(mesh):
    torus = Mesh(
        mesh.devices.reshape(mesh.shape["rep"], 2, 4, 4, mesh.shape["tp"]),
        ("rep", "fs_0", "fs_1", "fs_2", "tp"),
    )
    in_specs = (
        P(REP_FS, "tp"),
        P(),
        P(),
        P(),
        P(FS, "tp"),
        P(FS, "tp"),
        P("tp", FS),
        P("tp"),
        P("tp"),
        P(FS),
        P(FS, "tp"),
        P(FS, "tp"),
        P("tp"),
        P("tp"),
        P("tp"),
        P("tp"),
        P("tp", None, None),
        P("tp", None),
        P("tp", FS),
        P(FS),
    )
    out_specs = P(REP_FS, "tp")
    return jax.shard_map(
        on_device, mesh=torus, in_specs=in_specs, out_specs=out_specs, check_vma=False
    )
```

time: 243 us -> 244 us (level)
  Pallas kernels: 0 us -> 69.4 us
  matrix products: 60.2 us -> 0 us
  other arithmetic: 20.5 us -> 8.84 us
    pallas_call x0 -> x4, Pallas kernels: none -> 69.4 us  [the longest x1 26.7 us: second_pass(): pl.pallas_call(functools.partial(second_kernel, tiles, sent), out_shape=[...]
    dot_general x7 -> x0, matrix products: 60.2 us -> none  [the longest x3 38.4 us: times_rows(): lax.dot_general(left, rows, (((1,), (1,)), ((), ())), preferred_element_t...]
    select_n x6 -> x0, other arithmetic: 6.68 us -> none  [the longest x3 4.13 us: spread_sum(): arrived = other_core(jnp.where(first_core, right, left))]
    unnamed x34 -> x13, local copies, waits for them, and re-layouts: 0.92 us -> 4.44 us
    convert_element_type x4 -> x1, other arithmetic: 6.68 us -> 3.65 us  [on_device(): return (base.astype(jnp.float32) + 0.5 * last).astype(low)]
    all_gather x1, waiting for transfers between devices: 124 us -> 127 us  [on_device(): both = lax.all_gather(mine, REP_FS, axis=0, tiled=True)]
    ppermute x7 -> x5, starting transfers between devices: 4.95 us -> 3.56 us  [other_core(): return lax.ppermute(x, 'tp', [(0, 1), (1, 0)])]
    ppermute x7 -> x5, waiting for transfers between devices: 16.7 us -> 15.8 us  [other_core(): return lax.ppermute(x, 'tp', [(0, 1), (1, 0)])]
  transfers between devices with their start and end apart: 8 -> 6, of which waited for: 8 -> 6; matrix products, arithmetic and copies ran while one was open for 1% -> 0% of each run, Pallas kernels for 0% -> 0%
where the time goes in v2:
time: 244 us; the launch traced here: 243 us
  waiting for transfers between devices  143 us (59%)
  Pallas kernels  69.4 us (28%)
  between operations  13.4 us (5%)
  other arithmetic  8.84 us (4%)
  local copies, waits for them, and re-layouts  4.45 us (2%)
  starting transfers between devices  3.57 us (1%)
    all_gather x1, waiting for transfers between devices, on_device(): both = lax.all_gather(mine, REP_FS, axis=0, tiled=True)  127 us
    pallas_call x1, Pallas kernels, second_pass(): pl.pallas_call(functools.partial(second_kernel, tiles, sent), out_shape=[...  26.7 us
    pallas_call x1, Pallas kernels, first_pass(): pl.pallas_call(functools.partial(first_kernel, tiles), out_shape=jax.Shap...  23.7 us
    ppermute x5, waiting for transfers between devices, other_core(): return lax.ppermute(x, 'tp', [(0, 1), (1, 0)])  15.8 us
    pallas_call x1, Pallas kernels, gates(): pl.pallas_call(gates_kernel, out_shape=[jax.ShapeDtypeStruct((count, widt...  10.5 us
    pallas_call x1, Pallas kernels, mix(): pl.pallas_call(mix_kernel, out_shape=jax.ShapeDtypeStruct((count, width),...  8.44 us
  transfers between devices with their start and end apart: 6, of which 6 were waited for; matrix products, arithmetic and copies ran while one was open for 0% of the time, Pallas kernels for 0%

profile of v2, /device:TPU:1, one launch (start us, length us, event | category | flops | bytes accessed | tf_op | source)
XLA Modules:
  0.0 242.5 jit_solution(16494121229535756178)
XLA Ops:
  6.5 0.0 all-gather.2.cloned.1.call-start
  6.5 1.2 fusion
  7.7 1.0 fusion.1
  8.7 1.2 multiply_convert_fusion
  9.9 1.0 multiply_convert_fusion.4
  10.9 0.9 maximum_select_fusion
  11.8 0.0 all-gather.2.cloned.1.call-update
  11.8 0.0 copy-done
  11.8 1.5 collective-permute-start
  13.3 2.7 %collective-permute-done.other = bf16[640,1024]{1,0:T(8,128)(2,1)S(1)} collective-permute-done((bf16[640,1024]{1,0:T(8,128)(2,1)S(1)}, bf16[640,1024]{1,0:T(8,128)(2,1)S(1)}, u32[]{:S(2)}, u32[]{:S(2)}) %collective-permute-start) | collective-permute-done | bytes 1310752 | tf_op jit(solution)/shard_map/ppermute | solution.py:22
  15.9 0.0 copy-start.1
  15.9 127.1 %all-gather.2.cloned.1.call-done = bf16[4096,2944]{1,0:T(8,128)(2,1)} async-done(((bf16[64,2944]{1,0:T(8,128)(2,1)}), bf16[4096,2944]{1,0:T(8,128)(2,1)}) %all-gather.2.cloned.1.call-update) | async-done | bytes 24117264 | tf_op jit(solution)/shard_map/all_gather | solution.py:343
  143.0 0.0 copy-done.1
  143.0 23.7 %first_pass.1.term = bf16[640,2048]{1,0:T(8,128)(2,1)} custom-call(s32[1]{0:T(128)} %bitcast.core, bf16[640,1024]{1,0:T(8,128)(2,1)} %own.3, bf16[640,1024]{1,0:T(8,128)(2,1)} %copy-done.1, f32[1,2048]{1,0:T(1,128)} %bitcast.22, bf16[2,2048,2944]{2,1,0:T(8,128)(2,1)} %bitcast.12, bf16[2,2048,2944]{2,1,0:T(8,128)(2,1)} %bitcast.13, ...), custom_call_target="tpu_custom_call" | custom-call | flops 11072962560 | bytes 17301504 | tf_op jit(solution)/shard_map/first_pass/pallas_call | solution.py:94
  166.7 0.8 collective-permute-start.1
  167.5 4.7 %collective-permute-done.1.far = bf16[640,2048]{1,0:T(8,128)(2,1)S(1)} collective-permute-done((bf16[640,2048]{1,0:T(8,128)(2,1)}, bf16[640,2048]{1,0:T(8,128)(2,1)S(1)}, u32[]{:S(2)}, u32[]{:S(2)}) %collective-permute-start.1) | collective-permute-done | bytes 2621472 | tf_op jit(solution)/shard_map/ppermute | solution.py:22
  172.3 0.0 copy-start.3
  172.3 1.5 copy-done.3
  173.7 10.5 %gates.1 = (bf16[640,2048]{1,0:T(8,128)(2,1)}, f32[640,512]{1,0:T(8,128)}, f32[640,512]{1,0:T(8,128)}, f32[640,128]{1,0:T(8,128)}) custom-call(s32[1]{0:T(128)} %bitcast.core, bf16[640,1024]{1,0:T(8,128)(2,1)} %own.3, bf16[640,1024]{1,0:T(8,128)(2,1)} %copy-done.1, bf16[640,2048]{1,0:T(8,128)(2,1)} %first_pass.1.term, bf16[640,2048]{1,0:T(8,128)(2,1)} %copy-done.3, ...), custom_call_target="tpu_custom_call" | custom-call | flops 2684354560 | bytes 4194304 | tf_op jit(solution)/shard_map/gates/pallas_call | solution.py:221
  184.3 0.4 collective-permute-start.2
  184.7 0.0 copy-done.5
  184.7 0.7 copy.21
  185.5 0.7 collective-permute-done.2.far
  186.2 0.7 copy-done.4
  186.9 8.4 %mix.1.term = bf16[640,2048]{1,0:T(8,128)(2,1)} custom-call(f32[640,512]{1,0:T(8,128)} %get-tuple-element.13.u_act, f32[640,512]{1,0:T(8,128)} %get-tuple-element.14.v_act, f32[640,128]{1,0:T(8,128)} %get-tuple-element.15.sums, f32[640,128]{1,0:T(8,128)} %copy-done.4, f32[1,512]{1,0:T(1,128)} %bitcast.25, f32[1,512]{1,0:T(1,128)} %bitcast.26, ...), custom_call_target="tpu_custom_call" | custom-call | flops 1342177280 | bytes 2097152 | tf_op jit(solution)/shard_map/mix/pallas_call | solution.py:281
  195.4 0.4 collective-permute-start.3
  195.7 4.7 %collective-permute-done.3.far = bf16[640,2048]{1,0:T(8,128)(2,1)S(1)} collective-permute-done((bf16[640,2048]{1,0:T(8,128)(2,1)}, bf16[640,2048]{1,0:T(8,128)(2,1)S(1)}, u32[]{:S(2)}, u32[]{:S(2)}) %collective-permute-start.3) | collective-permute-done | bytes 2621472 | tf_op jit(solution)/shard_map/ppermute | solution.py:22
  200.5 1.5 copy-done.2
  202.0 26.7 %second_pass.1 = (bf16[640,1024]{1,0:T(8,128)(2,1)}, bf16[640,1024]{1,0:T(8,128)(2,1)}, bf16[640,1024]{1,0:T(8,128)(2,1)}) custom-call(s32[1]{0:T(128)} %bitcast.core, bf16[640,2048]{1,0:T(8,128)(2,1)} %get-tuple-element.12.middle, bf16[640,2048]{1,0:T(8,128)(2,1)} %mix.1.term, bf16[640,2048]{1,0:T(8,128)(2,1)} %copy-done.2, f32[1,2048]{1,0:T(1,128)} %bitcast.24, ...), custom_call_target="tpu_custom_call" | custom-call | flops 11072962560 | bytes 17301504 | tf_op jit(solution)/shard_map/second_pass/pallas_call | solution.py:165
  228.7 0.5 collective-permute-start.4
  229.1 2.9 %collective-permute-done.4 = bf16[640,1024]{1,0:T(8,128)(2,1)S(1)} collective-permute-done((bf16[640,1024]{1,0:T(8,128)(2,1)}, bf16[640,1024]{1,0:T(8,128)(2,1)S(1)}, u32[]{:S(2)}, u32[]{:S(2)}) %collective-permute-start.4) | collective-permute-done | bytes 1310752 | tf_op jit(solution)/shard_map/ppermute | solution.py:22
  232.0 3.6 %add_convert_fusion = bf16[640,1024]{1,0:T(8,128)(2,1)} fusion(bf16[640,1024]{1,0:T(8,128)(2,1)S(1)} %collective-permute-done.4, bf16[640,1024]{1,0:T(8,128)(2,1)} %get-tuple-element.17, bf16[640,1024]{1,0:T(8,128)(2,1)} %get-tuple-element.16), kind=kLoop, calls=%fused_computation | loop fusion | flops 4587520 | bytes 5242880 | tf_op jit(solution)/shard_map/convert_element_type | solution.py:364
  (6 shorter events, 0.0 us)
Async XLA Ops:
  6.5 5.3 %copy-start = (bf16[640,1024]{1,0:T(8,128)(2,1)S(1)}, bf16[640,1024]{1,0:T(8,128)(2,1)}, u32[]{:S(2)}) copy-start(bf16[640,1024]{1,0:T(8,128)(2,1)} %own.3) | copy-start | bytes 3932164
  6.5 136.5 %all-gather.2.cloned.1.call-start = ((), (), s32[]{:S(2)}) async-start(), calls=%async_computation | async-start | bytes 24494080 | tf_op jit(solution)/shard_map/all_gather | solution.py:343
  11.8 4.1 %collective-permute-start = (bf16[640,1024]{1,0:T(8,128)(2,1)S(1)}, bf16[640,1024]{1,0:T(8,128)(2,1)S(1)}, u32[]{:S(2)}, u32[]{:S(2)}) collective-permute-start(bf16[640,1024]{1,0:T(8,128)(2,1)S(1)} %copy-done), channel_id=1, source_target_pairs={{0,1},{1,0},{2,3},{3,2},{4,5},{5,4},{6,7},{7,6},{8,9},{9,8},{10,11... | collective-permute-start | bytes 3932168 | tf_op jit(solution)/shard_map/ppermute | solution.py:22
  15.9 127.1 %copy-start.1 = (bf16[640,1024]{1,0:T(8,128)(2,1)}, bf16[640,1024]{1,0:T(8,128)(2,1)S(1)}, u32[]{:S(2)}) copy-start(bf16[640,1024]{1,0:T(8,128)(2,1)S(1)} %collective-permute-done.other) | copy-start | bytes 3932164
  166.7 5.6 %collective-permute-start.1 = (bf16[640,2048]{1,0:T(8,128)(2,1)}, bf16[640,2048]{1,0:T(8,128)(2,1)S(1)}, u32[]{:S(2)}, u32[]{:S(2)}) collective-permute-start(bf16[640,2048]{1,0:T(8,128)(2,1)} %first_pass.1.term), channel_id=1, source_target_pairs={{0,1},{1,0},{2,3},{3,2},{4,5},{5,4},{6,7},{7,6},{8,9},{9,8},{10,11... | collective-permute-start | bytes 7864328 | tf_op jit(solution)/shard_map/ppermute | solution.py:22
  172.3 1.5 copy-start.3
  173.7 11.0 %copy-start.5 = (f32[4,128]{1,0:T(4,128)S(1)}, f32[4,128]{1,0:T(4,128)}, u32[]{:S(2)}) copy-start(f32[4,128]{1,0:T(4,128)} %param.37) | copy-start | bytes 6148
  184.3 1.9 collective-permute-start.2
  186.2 0.7 copy-start.4
  195.4 5.1 %collective-permute-start.3 = (bf16[640,2048]{1,0:T(8,128)(2,1)}, bf16[640,2048]{1,0:T(8,128)(2,1)S(1)}, u32[]{:S(2)}, u32[]{:S(2)}) collective-permute-start(bf16[640,2048]{1,0:T(8,128)(2,1)} %mix.1.term), channel_id=1, source_target_pairs={{0,1},{1,0},{2,3},{3,2},{4,5},{5,4},{6,7},{7,6},{8,9},{9,8},{10,11... | collective-permute-start | bytes 7864328 | tf_op jit(solution)/shard_map/ppermute | solution.py:22
  200.5 1.5 copy-start.2
  228.7 3.3 %collective-permute-start.4 = (bf16[640,1024]{1,0:T(8,128)(2,1)}, bf16[640,1024]{1,0:T(8,128)(2,1)S(1)}, u32[]{:S(2)}, u32[]{:S(2)}) collective-permute-start(bf16[640,1024]{1,0:T(8,128)(2,1)} %get-tuple-element.18), channel_id=1, source_target_pairs={{0,1},{1,0},{2,3},{3,2},{4,5},{5,4},{6,7},{7,6},{8,9},{9,8},{10,11... | collective-permute-start | bytes 3932168 | tf_op jit(solution)/shard_map/ppermute | solution.py:22
Sparse Core Ops, SparseCore 0:
  11.9 131.0 all-gather.1
